TPU v7x, 256 devices: a 4x2x16 block of a 4x16x16 slice. The times are simulated.
256 devices in a mesh: grp: 2 (over y), sp: 32 (over z, core), tp: 4 (over x).
Axes of the slice: x: 4, y: 2, z: 16, core: 2. Of those that a mesh axis runs over, the one named last changes fastest.
The devices are a block of a 4x16x16 slice.
Arguments:
- query_wide: bfloat16 [32768, 1024], P(('grp', 'sp'), 'tp'), parts along dimension 0, may hold values from -6 to 6
- key_wide: bfloat16 [32768, 1024], P(('grp', 'sp'), 'tp'), parts along dimension 0, may hold values from -6 to 6
- value_wide: bfloat16 [32768, 1024], P(('grp', 'sp'), 'tp'), parts along dimension 0, may hold values from -6 to 6
- decay_wide: float32 [32768, 8], P(('grp', 'sp'), 'tp'), parts along dimension 0, may hold values from -2 to 0, as said below
- query_narrow: bfloat16 [32768, 1024], P(('grp', 'sp'), 'tp'), parts along dimension 0, may hold values from -6 to 6
- key_narrow: bfloat16 [32768, 1024], P(('grp', 'sp'), 'tp'), parts along dimension 0, may hold values from -6 to 6
- value_narrow: bfloat16 [32768, 1024], P(('grp', 'sp'), 'tp'), parts along dimension 0, may hold values from -6 to 6
- decay_narrow: float32 [32768, 16], P(('grp', 'sp'), 'tp'), parts along dimension 0, may hold values from -2 to 0, as said below
- residual: bfloat16 [32768, 2048], P(('grp', 'sp', 'tp')), parts along dimension 0, may hold values from -6 to 6
- out_wide: bfloat16 [1024, 2048], P('tp'), may hold values from -0.125 to 0.125
- out_narrow: bfloat16 [1024, 2048], P('tp'), may hold values from -0.125 to 0.125
- norm_gain: float32 [2048], replicated, may hold values from 0.1 to 1.9
- routes: int32 [32768, 2], P(('grp', 'sp', 'tp')), parts along dimension 0, may hold values from 0 to 31, all different within a row; in each aligned block of 128 rows (0 to 127, 128 to 255, ...) at most 12 rows name the same one
- route_weights: float32 [32768, 2], P(('grp', 'sp', 'tp')), parts along dimension 0, may hold values from 0.1 to 1
- expert_gate: bfloat16 [32, 2048, 2048], P('sp', None, 'tp'), may hold values from -0.375 to 0.375
- expert_up: bfloat16 [32, 2048, 2048], P('sp', None, 'tp'), may hold values from -0.375 to 0.375
- expert_down: bfloat16 [32, 2048, 2048], P('sp', 'tp'), may hold values from -0.03125 to 0.03125
Outputs:
- layer_out: bfloat16 [32768, 2048], P(('grp', 'sp', 'tp')), parts along dimension 0
There are 2 independent parts, one for each index of `grp`. A program takes and returns all parts, laid end to end along the dimension named above; an argument that names none is the same for every part. Nothing has to cross between parts.
Inputs may be any that keep to these rules, and one draw needn't show every extreme that they name: `decay_wide`: every entry is negative. `decay_narrow`: every entry is negative. `routes`: each row names 2 different experts; on the rows of one device no expert is named more than 12 times, a bound that some block reaches.
All inputs are finite; a program needn't handle non-finite values.
Results may differ from a plain program's by a relative error of at most 0.018.
Values may be sent and summed in bfloat16 or wider, within the bound.
No kernel may reach another device: no remote copies, remote signals or barrier semaphores. Data moves between devices by JAX's collectives and lax.ppermute only.
A program may use at most 128 MiB of HBM per device.

v0:
```python
import jax
import jax.numpy as jnp
from jax import lax
from jax.sharding import Mesh
from jax.sharding import PartitionSpec as P

HEAD_WIDE = 128
HEAD_NARROW = 64
TOP_K = 2
SP = ("sp_0", "sp_1")
GRP_SP = ("grp", "sp_0", "sp_1")
GRP_SP_TP = ("grp", "sp_0", "sp_1", "tp")
norm_eps = 1e-05
clamp_limit = 7.0
swish_alpha = 1.702
rotary_base = 10000.0


def filled_with(value, identity):
    return jax.tree.map(
        lambda a, e: jnp.broadcast_to(jnp.asarray(e, a.dtype), a.shape), value, identity
    )


def prefix_by_axis(value, axes, combine, identity):
    before = start = filled_with(value, identity)
    total = value
    for axis in reversed(axes):
        length, mine = (lax.axis_size(axis), lax.axis_index(axis))
        pieces = jax.tree.map(
            lambda part, kind: lax.all_gather(part.astype(kind), axis),
            total,
            jax.tree.map(lambda a: jnp.bfloat16 if a.dtype == jnp.float32 else a.dtype, value),
        )
        inside, total = (start, start)
        for k in range(length):
            passed = k < mine
            total = combine(
                total, jax.tree.map(lambda part, own: part[k].astype(own.dtype), pieces, value)
            )
            inside = jax.tree.map(lambda new, old: jnp.where(passed, new, old), total, inside)
        before = combine(inside, before)
    return before


def cut_along(value, dim, length):
    lengths = value.shape
    pieces = value.reshape(*lengths[:dim], length, lengths[dim] // length, *lengths[dim + 1 :])
    return jnp.moveaxis(pieces, dim, 0)


def sent_and_summed(value, axis, dim):
    pieces = cut_along(value, dim, lax.axis_size(axis))
    arrived = lax.all_to_all(pieces, axis, split_axis=0, concat_axis=0, tiled=True)
    return arrived.astype(jnp.float32).sum(axis=0)


def laid_out(pieces, dim):
    pieces = jnp.moveaxis(pieces, 0, dim)
    lengths = pieces.shape
    return pieces.reshape(*lengths[:dim], lengths[dim] * lengths[dim + 1], *lengths[dim + 2 :])


def turned_blocks(pieces, axes, order):
    inside = pieces.shape[1:]
    filled = pieces.reshape(*(lax.axis_size(a) for a in axes), *inside)
    for k in order:
        filled = lax.all_to_all(filled, axes[k], k, k, tiled=True)
    return filled.reshape(-1, *inside)


def core_and_chips(value, groups, order, split_dim, concat_dim):
    length = lax.axis_size(groups[0]) * lax.axis_size(groups[1])
    pieces = cut_along(value, split_dim, length)
    return laid_out(turned_blocks(pieces, groups, order), concat_dim)


def rotate(values, positions):
    half_width = values.shape[-1] // 2
    inverse = rotary_base ** (-jnp.arange(half_width, dtype=jnp.float32) / half_width)
    angles = positions[:, None] * inverse[None, :]
    cosine = jnp.cos(angles)[:, None, :]
    sine_part = jnp.sin(angles)[:, None, :]
    lower_half = values[..., :half_width]
    upper_half = values[..., half_width:]
    return jnp.concatenate(
        [
            lower_half * cosine - upper_half * sine_part,
            lower_half * sine_part + upper_half * cosine,
        ],
        axis=-1,
    )


def group_norm(output_heads):
    center = jnp.mean(output_heads, axis=-1, keepdims=True)
    spread = jnp.mean(jnp.square(output_heads - center), axis=-1, keepdims=True)
    return (output_heads - center) * lax.rsqrt(spread + norm_eps)


def local_terms(query_in, key_in, value_in, log_decay, head_width, positions):
    length = query_in.shape[0]
    attention_group_count = query_in.shape[1] // head_width
    query_heads = query_in.astype(jnp.float32).reshape(length, attention_group_count, head_width)
    key_heads = key_in.astype(jnp.float32).reshape(length, attention_group_count, head_width)
    query_f = rotate(query_heads, positions).astype(jnp.bfloat16).astype(jnp.float32)
    key_f = (
        (rotate(key_heads, positions) * head_width ** (-0.5))
        .astype(jnp.bfloat16)
        .astype(jnp.float32)
    )
    value_f = value_in.reshape(length, attention_group_count, head_width).astype(jnp.float32)
    cumulative = jnp.cumsum(log_decay, axis=0)
    steps_in = jnp.arange(length, dtype=jnp.int32)
    causal = steps_in[:, None] >= steps_in[None, :]
    gaps = cumulative.T[:, :, None] - cumulative.T[:, None, :]
    decay_grid = jnp.exp(jnp.where(causal[None], gaps, -jnp.inf))
    scores = jnp.einsum("thd,shd->hts", query_f, key_f) * decay_grid
    inner_part = jnp.einsum("hts,she->the", scores, value_f)
    total_log = cumulative[-1]
    weighted = key_f * jnp.exp(total_log[None, :] - cumulative)[:, :, None]
    state_local = jnp.einsum("shd,she->hde", weighted, value_f)
    return (query_f, cumulative, inner_part, total_log, state_local)


def finish(parts, state_in):
    query_f, cumulative, inner_part = (parts[0], parts[1], parts[2])
    carried_part = jnp.exp(cumulative)[:, :, None] * jnp.einsum("thd,hde->the", query_f, state_in)
    normed_heads = group_norm(inner_part + carried_part)
    return normed_heads.reshape(normed_heads.shape[0], -1).astype(jnp.bfloat16)


def combine(earlier, later):
    return (
        earlier[0] + later[0],
        jnp.exp(later[0])[:, None, None] * earlier[1] + later[1],
        earlier[2] + later[2],
        jnp.exp(later[2])[:, None, None] * earlier[3] + later[3],
    )


def activate(gate_pre, up_pre):
    gate_clip = jnp.minimum(gate_pre, clamp_limit)
    up_clip = jnp.clip(up_pre, -clamp_limit, clamp_limit)
    return gate_clip * jax.nn.sigmoid(swish_alpha * gate_clip) * (up_clip + 1.0)


def body(
    query_wide,
    key_wide,
    value_wide,
    decay_wide,
    query_narrow,
    key_narrow,
    value_narrow,
    decay_narrow,
    residual,
    out_wide,
    out_narrow,
    norm_gain,
    routes,
    route_weights,
    expert_gate,
    expert_up,
    expert_down,
):
    length = query_wide.shape[0]
    tp_count = lax.axis_size("tp")
    experts = lax.axis_size(SP)
    model_width = residual.shape[1]
    positions = (lax.axis_index(SP) * length + jnp.arange(length, dtype=jnp.int32)).astype(
        jnp.float32
    )
    wide_parts = local_terms(query_wide, key_wide, value_wide, decay_wide, HEAD_WIDE, positions)
    narrow_parts = local_terms(
        query_narrow, key_narrow, value_narrow, decay_narrow, HEAD_NARROW, positions
    )
    local_states = (wide_parts[3], wide_parts[4], narrow_parts[3], narrow_parts[4])
    identity = tuple((jnp.zeros_like(member) for member in local_states))
    carried = prefix_by_axis(local_states, SP, combine, identity)
    mixed_wide = finish(wide_parts, carried[1])
    mixed_narrow = finish(narrow_parts, carried[3])
    rows_dev = length // tp_count
    attention = sent_and_summed(
        (
            jnp.dot(mixed_wide, out_wide, preferred_element_type=jnp.float32)
            + jnp.dot(mixed_narrow, out_narrow, preferred_element_type=jnp.float32)
        ).astype(jnp.bfloat16),
        "tp",
        0,
    )
    hidden_state = residual.astype(jnp.float32) + attention
    scale_row = lax.rsqrt(jnp.mean(hidden_state * hidden_state, axis=-1, keepdims=True) + norm_eps)
    normed = (hidden_state * scale_row * norm_gain).astype(jnp.bfloat16)
    capacity = max(2, 3 * rows_dev * TOP_K // (2 * experts))
    flat_expert = routes.reshape(-1)
    one_hot = (flat_expert[:, None] == jnp.arange(experts, dtype=jnp.int32)[None, :]).astype(
        jnp.int32
    )
    rank_in = jnp.sum((jnp.cumsum(one_hot, axis=0) - one_hot) * one_hot, axis=1)
    slot_index = flat_expert * capacity + rank_in
    source_row = jnp.arange(rows_dev * TOP_K, dtype=jnp.int32) // TOP_K
    slot_table = jnp.zeros((experts * capacity,), jnp.int32).at[slot_index].set(source_row + 1)
    padded = jnp.concatenate([jnp.zeros((1, model_width), jnp.bfloat16), normed], axis=0)
    send_slots = padded[slot_table].reshape(experts, capacity, model_width)
    gate_shard = expert_gate[0]
    up_shard = expert_up[0]
    down_shard = expert_down[0]
    gathered = lax.all_gather(
        core_and_chips(send_slots, ("sp_0", "sp_1"), (1, 0), 0, 0), "tp", axis=0, tiled=True
    )
    flat_rows = gathered.reshape(-1, model_width)
    gate_pre = jnp.dot(flat_rows, gate_shard, preferred_element_type=jnp.float32)
    up_pre = jnp.dot(flat_rows, up_shard, preferred_element_type=jnp.float32)
    hidden = activate(gate_pre, up_pre).astype(jnp.bfloat16)
    partial_value = jnp.dot(hidden, down_shard, preferred_element_type=jnp.float32)
    partial_value = partial_value.reshape(gathered.shape[0], gathered.shape[1], model_width)
    summed = sent_and_summed(
        partial_value.reshape(tp_count, experts, capacity, model_width).astype(jnp.bfloat16),
        "tp",
        0,
    )
    expert_output = summed.reshape(experts, capacity, model_width).astype(jnp.bfloat16)
    returned = lax.all_to_all(expert_output, SP, split_axis=0, concat_axis=0, tiled=True)
    picked = returned.reshape(experts * capacity, model_width)[slot_index].astype(jnp.float32)
    routed = jnp.sum(
        (picked * route_weights.reshape(-1)[:, None]).reshape(rows_dev, TOP_K, model_width), axis=1
    )
    return (hidden_state + routed).astype(jnp.bfloat16)


def solution(mesh):
    torus = Mesh(
        mesh.devices.reshape(mesh.shape["grp"], 16, 2, mesh.shape["tp"]),
        ("grp", "sp_0", "sp_1", "tp"),
    )
    in_specs = (
        P(GRP_SP, "tp"),
        P(GRP_SP, "tp"),
        P(GRP_SP, "tp"),
        P(GRP_SP, "tp"),
        P(GRP_SP, "tp"),
        P(GRP_SP, "tp"),
        P(GRP_SP, "tp"),
        P(GRP_SP, "tp"),
        P(GRP_SP_TP, None),
        P("tp", None),
        P("tp", None),
        P(),
        P(GRP_SP_TP, None),
        P(GRP_SP_TP, None),
        P(SP, None, "tp"),
        P(SP, None, "tp"),
        P(SP, "tp", None),
    )
    out_specs = P(GRP_SP_TP, None)
    return jax.shard_map(body, mesh=torus, in_specs=in_specs, out_specs=out_specs, check_vma=False)
```

profile of v0, /device:TPU:33, one launch (start us, length us, event | category | flops | bytes accessed | tf_op | source)
XLA Modules:
  0.0 619.4 jit_solution(2552972941295234430)
XLA Ops:
  23.0 22.0 %all-gather = bf16[4,128,128]{2,1,0:T(8,128)(2,1)S(1)} all-gather(bf16[2,128,128]{2,1,0:T(8,128)(2,1)S(1)} %convolution_convert_fusion.1), channel_id=2, replica_groups=mesh['grp'=2,'sp_0'=16,'sp_1'=2,'tp'=4] {'sp_1'}, dimensions={0}, use_global_device_ids=true | all-gather | bytes 196608 | tf_op jit(solution)/shard_map/all_gather | solution.py:31
  60.3 32.4 %all_gather.48 = bf16[16,4,64,64]{3,2,1,0:T(8,128)(2,1)S(1)} all-gather(bf16[1,4,64,64]{3,2,1,0:T(8,128)(2,1)S(1)} %fusion.70), channel_id=1, replica_groups=mesh['grp'=2,'sp_0'=16,'sp_1'=2,'tp'=4] {'sp_0'}, dimensions={0}, use_global_device_ids=true | all-gather | bytes 557056 | tf_op jit(solution)/shard_map/all_gather | solution.py:31
  92.8 21.5 %all-gather.5 = bf16[16,1,4]{2,1,0:T(2,128)(2,1)S(1)} all-gather(bf16[1,1,4]{2,1,0:T(2,128)(2,1)S(1)} %get-tuple-element.65), channel_id=1, replica_groups=mesh['grp'=2,'sp_0'=16,'sp_1'=2,'tp'=4] {'sp_0'}, dimensions={0}, use_global_device_ids=true | all-gather | bytes 136 | tf_op jit(solution)/shard_map/all_gather | solution.py:31
  115.0 19.9 %all-gather.3 = bf16[16,1,2]{2,1,0:T(2,128)(2,1)S(1)} all-gather(bf16[1,1,2]{2,1,0:T(2,128)(2,1)} %get-tuple-element.68), channel_id=1, replica_groups=mesh['grp'=2,'sp_0'=16,'sp_1'=2,'tp'=4] {'sp_0'}, dimensions={0}, use_global_device_ids=true | all-gather | bytes 68 | tf_op jit(solution)/shard_map/all_gather | solution.py:31
  136.3 4.1 fusion.31
  152.4 4.7 all-to-all-start
  160.2 12.2 %all-to-all-done = bf16[4,128,2048]{2,1,0:T(8,128)(2,1)} async-done(((bf16[4,128,2048]{2,1,0:T(8,128)(2,1)}), bf16[4,128,2048]{2,1,0:T(8,128)(2,1)}, u32[]{:S(2)}, u32[]{:S(2)}) %all-to-all-start) | async-done | bytes 2097184 | tf_op jit(solution)/shard_map/all_to_all | solution.py:54
  179.0 3.6 reshape_reshape_reshape.3
  185.1 24.8 %all_to_all.25 = bf16[16,2,1,12,2048]{4,0,3,2,1:T(8,128)(2,1)S(1)} all-to-all(bf16[16,2,1,12,2048]{4,0,3,2,1:T(8,128)(2,1)S(1)} %copy.204), channel_id=1, replica_groups=mesh['grp'=2,'sp_0'=16,'sp_1'=2,'tp'=4] {'sp_1'}, dimensions={1} | all-to-all | bytes 3145728 | tf_op jit(solution)/shard_map/all_to_all | solution.py:68
  211.5 72.3 %all_to_all.26 = bf16[16,2,1,12,2048]{4,1,3,2,0:T(2,128)(2,1)S(1)} all-to-all(bf16[16,2,1,12,2048]{4,1,3,2,0:T(2,128)(2,1)S(1)} %copy.205), channel_id=1, replica_groups=mesh['grp'=2,'sp_0'=16,'sp_1'=2,'tp'=4] {'sp_0'}, dimensions={0} | all-to-all | bytes 3145728 | tf_op jit(solution)/shard_map/all_to_all | solution.py:68
  286.4 3.7 reshape_reshape.4
  290.1 72.6 %all-gather.11.cloned.1.call-done = bf16[128,12,2048]{2,0,1:T(8,128)(2,1)} async-done(((bf16[32,12,2048]{2,0,1:T(8,128)(2,1)}), bf16[128,12,2048]{2,0,1:T(8,128)(2,1)}) %all-gather.11.cloned.1.call-update) | async-done | bytes 6291472 | tf_op jit(solution)/shard_map/all_gather | solution.py:209
  362.7 9.7 %copy.207 = bf16[128,12,2048]{2,1,0:T(8,128)(2,1)} copy(bf16[128,12,2048]{2,0,1:T(8,128)(2,1)} %all-gather.11.cloned.1.call-done) | data formatting | bytes 12582912 | tf_op jit(solution)/shard_map/all_gather | solution.py:209
  372.3 10.7 %reshape.746 = bf16[1536,2048]{1,0:T(8,128)(2,1)} reshape(bf16[128,12,2048]{2,1,0:T(8,128)(2,1)} %copy.207) | data formatting | bytes 12582912 | tf_op jit(solution)/shard_map/reshape | solution.py:212
  383.1 6.3 %convolution_minimum_fusion = f32[1536,512]{1,0:T(8,128)S(1)} fusion(bf16[1536,2048]{1,0:T(8,128)(2,1)} %reshape.746, bf16[1,2048,512]{2,1,0:T(8,128)(2,1)} %param.31), kind=kOutput, calls=%fused_computation.13 | convolution fusion | flops 3222011904 | bytes 11534336 | tf_op jit(solution)/shard_map/dot_general | solution.py:213
  389.4 5.0 fusion.7
  394.4 3.6 dot_general.53
  398.0 6.1 convert_bitcast_fusion
  404.1 73.7 %all_to_all.27 = bf16[4,1,32,12,2048]{4,2,3,1,0:T(8,128)(2,1)S(1)} all-to-all(bf16[4,1,32,12,2048]{4,2,3,1,0:T(8,128)(2,1)S(1)} %convert_bitcast_fusion), channel_id=1, replica_groups=mesh['grp'=2,'sp_0'=16,'sp_1'=2,'tp'=4] {'tp'}, dimensions={0} | all-to-all | bytes 12582912 | tf_op jit(solution)/shard_map/all_to_all | solution.py:54
  481.3 14.4 %all-to-all-start.4 = ((bf16[32,12,2048]{2,1,0:T(8,128)(2,1)}), bf16[32,12,2048]{2,1,0:T(8,128)(2,1)}, u32[]{:S(2)}, u32[]{:S(2)}) async-start(bf16[32,12,2048]{2,1,0:T(8,128)(2,1)} %copy.211), calls=%async_computation.4 | async-start | bytes 4194304 | tf_op jit(solution)/shard_map/all_to_all | solution.py:224
  495.9 98.6 %all-to-all-done.4 = bf16[32,12,2048]{2,1,0:T(8,128)(2,1)} async-done(((bf16[32,12,2048]{2,1,0:T(8,128)(2,1)}), bf16[32,12,2048]{2,1,0:T(8,128)(2,1)}, u32[]{:S(2)}, u32[]{:S(2)}) %all-to-all-start.4) | async-done | bytes 1572896 | tf_op jit(solution)/shard_map/all_to_all | solution.py:224
  594.4 3.6 reshape.748
  598.0 4.9 gather_fusion.1
  606.4 4.9 multiply_reduce_fusion
  (167 shorter events, 69.7 us)
Async XLA Ops:
  6.5 391.5 %copy-start = (bf16[1,512,2048]{2,1,0:T(8,128)(2,1)S(1)}, bf16[1,512,2048]{2,1,0:T(8,128)(2,1)}, u32[]{:S(2)}) copy-start(bf16[1,512,2048]{2,1,0:T(8,128)(2,1)} %param.33) | copy-start | bytes 6291460
  6.6 136.0 %all-gather.9.cloned.1.call-start = ((), (), s32[]{:S(2)}) async-start(), calls=%async_computation.5 | async-start | bytes 1114112 | tf_op jit(solution)/shard_map/all_gather | solution.py:31
  22.3 26.0 %copy-start.18 = (f32[512,4]{0,1:T(4,128)S(1)}, f32[512,4]{0,1:T(4,128)}, u32[]{:S(2)}) copy-start(f32[512,4]{0,1:T(4,128)} %param.24) | copy-start | bytes 24580
  22.3 29.9 %copy-start.6 = (bf16[512,256]{1,0:T(8,128)(2,1)S(1)}, bf16[512,256]{1,0:T(8,128)(2,1)}, u32[]{:S(2)}) copy-start(bf16[512,256]{1,0:T(8,128)(2,1)} %param.21) | copy-start | bytes 786436
  22.3 30.0 %copy-start.7 = (bf16[512,256]{1,0:T(8,128)(2,1)S(1)}, bf16[512,256]{1,0:T(8,128)(2,1)}, u32[]{:S(2)}) copy-start(bf16[512,256]{1,0:T(8,128)(2,1)} %param.22) | copy-start | bytes 786436
  22.5 29.6 %copy-start.10 = (bf16[512,2,128]{2,0,1:T(8,128)(2,1)}, bf16[512,2,128]{2,0,1:T(8,128)(2,1)S(1)}, u32[]{:S(2)}) copy-start(bf16[512,2,128]{2,0,1:T(8,128)(2,1)S(1)} %fusion.41) | copy-start | bytes 786436
  54.2 82.1 %copy-start.16 = (f32[1,4,4,128]{3,1,2,0:T(4,128)S(1)}, f32[1,4,4,128]{3,1,2,0:T(4,128)}, u32[]{:S(2)}) copy-start(f32[1,4,4,128]{3,1,2,0:T(4,128)} %copy-done.15) | copy-start | bytes 24580
  56.0 4.3 copy-start.11
  56.0 4.4 copy-start.12
  60.2 76.1 %copy-start.28 = (f32[4]{0:T(128)}, f32[4]{0:T(128)S(1)}, u32[]{:S(2)}) copy-start(f32[4]{0:T(128)S(1)} %get-tuple-element.66) | copy-start | bytes 52
  60.2 76.0 %copy-start.29 = (f32[4]{0:T(128)}, f32[4]{0:T(128)S(1)}, u32[]{:S(2)}) copy-start(f32[4]{0:T(128)S(1)} %get-tuple-element.67) | copy-start | bytes 52
  136.3 4.1 copy-start.14
  142.4 3.2 copy-start.8
  142.4 3.2 copy-start.9
  152.4 4.8 copy-start.19
  152.4 20.0 %all-to-all-start = ((bf16[4,128,2048]{2,1,0:T(8,128)(2,1)}), bf16[4,128,2048]{2,1,0:T(8,128)(2,1)}, u32[]{:S(2)}, u32[]{:S(2)}) async-start(bf16[4,128,2048]{2,1,0:T(8,128)(2,1)} %bitcast.468), calls=%async_computation | async-start | bytes 4194304 | tf_op jit(solution)/shard_map/all_to_all | solution.py:54
  157.1 17.5 %copy-start.4 = (bf16[128,2048]{1,0:T(8,128)(2,1)S(1)}, bf16[128,2048]{1,0:T(8,128)(2,1)}, u32[]{:S(2)}) copy-start(bf16[128,2048]{1,0:T(8,128)(2,1)} %param.25) | copy-start | bytes 1572868
  157.1 205.6 %all-gather.11.cloned.1.call-start = ((), (), s32[]{:S(2)}) async-start(), calls=%async_computation.6 | async-start | bytes 7864320 | tf_op jit(solution)/shard_map/all_gather | solution.py:209
  160.2 15.3 %copy-start.17 = (f32[2048]{0:T(1024)S(1)}, f32[2048]{0:T(1024)}, u32[]{:S(2)}) copy-start(f32[2048]{0:T(1024)} %param.28) | copy-start | bytes 24580
  383.1 6.3 %copy-start.3 = (bf16[1536,2048]{1,0:T(8,128)(2,1)S(1)}, bf16[1536,2048]{1,0:T(8,128)(2,1)}, u32[]{:S(2)}) copy-start(bf16[1536,2048]{1,0:T(8,128)(2,1)} %reshape.746) | copy-start | bytes 18874372
  383.1 6.3 %copy-start.31 = (bf16[1,2048,512]{2,1,0:T(8,128)(2,1)S(1)}, bf16[1,2048,512]{2,1,0:T(8,128)(2,1)}, u32[]{:S(2)}) copy-start(bf16[1,2048,512]{2,1,0:T(8,128)(2,1)} %param.32) | copy-start | bytes 6291460
  481.3 14.4 %copy-start.30 = (f32[128,2]{0,1:T(2,128)S(1)}, f32[128,2]{0,1:T(2,128)}, u32[]{:S(2)}) copy-start(f32[128,2]{0,1:T(2,128)} %param.30) | copy-start | bytes 3076
  481.3 113.1 %all-to-all-start.4 = ((bf16[32,12,2048]{2,1,0:T(8,128)(2,1)}), bf16[32,12,2048]{2,1,0:T(8,128)(2,1)}, u32[]{:S(2)}, u32[]{:S(2)}) async-start(bf16[32,12,2048]{2,1,0:T(8,128)(2,1)} %copy.211), calls=%async_computation.4 | async-start | bytes 4194304 | tf_op jit(solution)/shard_map/all_to_all | solution.py:224
  606.4 4.9 copy-start.2
  (13 other events, 23.4 us)
Sparse Core Ops, SparseCore 0:
  48.3 54.4 all-gather.8
  290.2 72.4 all-gather.10
where the time goes:
time: 626 us; the launch traced here: 619 us
  blocking collectives  273 us (44%)
  waiting for transfers between devices  184 us (29%)
  local copies, waits for them, and re-layouts  72.1 us (12%)
  matrix products  33.7 us (5%)
  other arithmetic  24.1 us (4%)
  starting transfers between devices  19.1 us (3%)
  between operations  14.3 us (2%)
    all_gather x7, blocking collectives, prefix_by_axis(): lax.all_gather(part.astype(kind), axis)  102 us
    all_to_all x1, waiting for transfers between devices, body(): lax.all_to_all(expert_output, SP, split_axis=0, concat_axis=0, tiled=True)  98.6 us
    all_to_all x2, blocking collectives, turned_blocks(): filled = lax.all_to_all(filled, axes[k], k, k, tiled=True)  97.1 us
    all_to_all x1, blocking collectives, sent_and_summed(): lax.all_to_all(pieces, axis, split_axis=0, concat_axis=0, tiled=True)  73.7 us
    all_gather x1, waiting for transfers between devices, body(): lax.all_gather(core_and_chips(send_slots, ('sp_0', 'sp_1'), (1, 0), 0, 0)...  72.6 us
    all_to_all x1, starting transfers between devices, body(): lax.all_to_all(expert_output, SP, split_axis=0, concat_axis=0, tiled=True)  14.4 us
  transfers between devices with their start and end apart: 4, of which 3 were waited for; matrix products, arithmetic and copies ran while one was open for 3% of the time, Pallas kernels for 0%

commit v1 on v0

--- a/solution.py
+++ b/solution.py
@@ -14,6 +14,11 @@
 clamp_limit = 7.0
 swish_alpha = 1.702
 rotary_base = 10000.0
+
+
+def gather_from_all(x, axis, dim):
+    copies = jnp.concatenate([x] * lax.axis_size(axis), axis=dim)
+    return lax.all_to_all(copies, axis, dim, dim, tiled=True)
 
 
 def filled_with(value, identity):
@@ -206,9 +211,7 @@
     gate_shard = expert_gate[0]
     up_shard = expert_up[0]
     down_shard = expert_down[0]
-    gathered = lax.all_gather(
-        core_and_chips(send_slots, ("sp_0", "sp_1"), (1, 0), 0, 0), "tp", axis=0, tiled=True
-    )
+    gathered = gather_from_all(core_and_chips(send_slots, ("sp_0", "sp_1"), (1, 0), 0, 0), "tp", 0)
     flat_rows = gathered.reshape(-1, model_width)
     gate_pre = jnp.dot(flat_rows, gate_shard, preferred_element_type=jnp.float32)
     up_pre = jnp.dot(flat_rows, up_shard, preferred_element_type=jnp.float32)

time: 626 us -> 659 us (1.053)
  blocking collectives: 273 us -> 359 us
  waiting for transfers between devices: 184 us -> 111 us
  starting transfers between devices: 19.1 us -> 34.5 us
    all_to_all x0 -> x1, blocking collectives: none -> 94.2 us  [gather_from_all(): return lax.all_to_all(copies, axis, dim, dim, tiled=True)]
    all_gather x1 -> x0, waiting for transfers between devices: 72.6 us -> none  [body(): lax.all_gather(core_and_chips(send_slots, ('sp_0', 'sp_1'), (1, 0), 0, 0)...]
    all_to_all x1, starting transfers between devices: 14.4 us -> 29.9 us  [body(): lax.all_to_all(expert_output, SP, split_axis=0, concat_axis=0, tiled=True)]
    all_gather x1 -> x0, local copies, waits for them, and re-layouts: 9.65 us -> none  [body(): lax.all_gather(core_and_chips(send_slots, ('sp_0', 'sp_1'), (1, 0), 0, 0)...]
    all_to_all x1, blocking collectives: 73.7 us -> 65.9 us  [sent_and_summed(): lax.all_to_all(pieces, axis, split_axis=0, concat_axis=0, tiled=True)]
    concatenate x0 -> x1, local copies, waits for them, and re-layouts: none -> 6.84 us  [gather_from_all(): copies = jnp.concatenate([x] * lax.axis_size(axis), axis=dim)]
  transfers between devices with their start and end apart: 4 -> 3, of which waited for: 3 -> 2; matrix products, arithmetic and copies ran while one was open for 3% -> 3% of each run, Pallas kernels for 0% -> 0%
where the time goes in v1:
time: 659 us; the launch traced here: 652 us
  blocking collectives  359 us (54%)
  waiting for transfers between devices  111 us (17%)
  local copies, waits for them, and re-layouts  71.1 us (11%)
  starting transfers between devices  34.5 us (5%)
  matrix products  33.7 us (5%)
  other arithmetic  29.4 us (4%)
  between operations  14.3 us (2%)
    all_gather x7, blocking collectives, prefix_by_axis(): lax.all_gather(part.astype(kind), axis)  101 us
    all_to_all x1, waiting for transfers between devices, body(): lax.all_to_all(expert_output, SP, split_axis=0, concat_axis=0, tiled=True)  98.1 us
    all_to_all x2, blocking collectives, turned_blocks(): filled = lax.all_to_all(filled, axes[k], k, k, tiled=True)  97.9 us
    all_to_all x1, blocking collectives, gather_from_all(): return lax.all_to_all(copies, axis, dim, dim, tiled=True)  94.2 us
    all_to_all x1, blocking collectives, sent_and_summed(): lax.all_to_all(pieces, axis, split_axis=0, concat_axis=0, tiled=True)  65.9 us
    all_to_all x1, starting transfers between devices, body(): lax.all_to_all(expert_output, SP, split_axis=0, concat_axis=0, tiled=True)  29.9 us
  transfers between devices with their start and end apart: 3, of which 2 were waited for; matrix products, arithmetic and copies ran while one was open for 3% of the time, Pallas kernels for 0%

profile of v1, /device:TPU:33, one launch (start us, length us, event | category | flops | bytes accessed | tf_op | source)
XLA Modules:
  0.0 652.4 jit_solution(16418877423427005246)
XLA Ops:
  23.6 22.0 %all-gather = bf16[4,128,128]{2,1,0:T(8,128)(2,1)S(1)} all-gather(bf16[2,128,128]{2,1,0:T(8,128)(2,1)S(1)} %convolution_convert_fusion.1), channel_id=2, replica_groups=mesh['grp'=2,'sp_0'=16,'sp_1'=2,'tp'=4] {'sp_1'}, dimensions={0}, use_global_device_ids=true | all-gather | bytes 196608 | tf_op jit(solution)/shard_map/all_gather | solution.py:36
  62.4 32.0 %all_gather.45 = bf16[16,4,64,64]{3,2,1,0:T(8,128)(2,1)S(1)} all-gather(bf16[1,4,64,64]{3,2,1,0:T(8,128)(2,1)S(1)} %fusion.70), channel_id=1, replica_groups=mesh['grp'=2,'sp_0'=16,'sp_1'=2,'tp'=4] {'sp_0'}, dimensions={0}, use_global_device_ids=true | all-gather | bytes 557056 | tf_op jit(solution)/shard_map/all_gather | solution.py:36
  94.4 20.6 %all-gather.5 = bf16[16,1,4]{2,1,0:T(2,128)(2,1)S(1)} all-gather(bf16[1,1,4]{2,1,0:T(2,128)(2,1)S(1)} %get-tuple-element.65), channel_id=1, replica_groups=mesh['grp'=2,'sp_0'=16,'sp_1'=2,'tp'=4] {'sp_0'}, dimensions={0}, use_global_device_ids=true | all-gather | bytes 136 | tf_op jit(solution)/shard_map/all_gather | solution.py:36
  115.7 20.7 %all-gather.3 = bf16[16,1,2]{2,1,0:T(2,128)(2,1)S(1)} all-gather(bf16[1,1,2]{2,1,0:T(2,128)(2,1)} %get-tuple-element.68), channel_id=1, replica_groups=mesh['grp'=2,'sp_0'=16,'sp_1'=2,'tp'=4] {'sp_0'}, dimensions={0}, use_global_device_ids=true | all-gather | bytes 68 | tf_op jit(solution)/shard_map/all_gather | solution.py:36
  137.8 4.1 fusion.31
  153.9 4.7 all-to-all-start
  161.7 12.3 %all-to-all-done = bf16[4,128,2048]{2,1,0:T(8,128)(2,1)} async-done(((bf16[4,128,2048]{2,1,0:T(8,128)(2,1)}), bf16[4,128,2048]{2,1,0:T(8,128)(2,1)}, u32[]{:S(2)}, u32[]{:S(2)}) %all-to-all-start) | async-done | bytes 2097184 | tf_op jit(solution)/shard_map/all_to_all | solution.py:59
  186.6 24.8 %all_to_all.30 = bf16[16,2,1,12,2048]{4,0,3,2,1:T(8,128)(2,1)S(1)} all-to-all(bf16[16,2,1,12,2048]{4,0,3,2,1:T(8,128)(2,1)S(1)} %copy.203), channel_id=1, replica_groups=mesh['grp'=2,'sp_0'=16,'sp_1'=2,'tp'=4] {'sp_1'}, dimensions={1} | all-to-all | bytes 3145728 | tf_op jit(solution)/shard_map/all_to_all | solution.py:73
  213.0 73.1 %all_to_all.31 = bf16[16,2,1,12,2048]{4,1,3,2,0:T(2,128)(2,1)S(1)} all-to-all(bf16[16,2,1,12,2048]{4,1,3,2,0:T(2,128)(2,1)S(1)} %copy.204), channel_id=1, replica_groups=mesh['grp'=2,'sp_0'=16,'sp_1'=2,'tp'=4] {'sp_0'}, dimensions={0} | all-to-all | bytes 3145728 | tf_op jit(solution)/shard_map/all_to_all | solution.py:73
  288.6 3.6 reshape_reshape.4
  292.3 4.8 pad_maximum_fusion
  297.1 6.8 %copy.206 = bf16[128,12,2048]{2,1,0:T(8,128)(2,1)} copy(bf16[128,12,2048]{2,0,1:T(8,128)(2,1)S(1)} %pad_maximum_fusion) | data formatting | bytes 12582912 | tf_op jit(solution)/shard_map/concatenate | solution.py:20
  304.0 94.2 %all_to_all.32 = bf16[128,12,2048]{2,1,0:T(8,128)(2,1)} all-to-all(bf16[128,12,2048]{2,1,0:T(8,128)(2,1)} %copy.206), channel_id=1, replica_groups=mesh['grp'=2,'sp_0'=16,'sp_1'=2,'tp'=4] {'tp'}, dimensions={0} | all-to-all | bytes 12582912 | tf_op jit(solution)/shard_map/all_to_all | solution.py:21
  398.2 10.7 %reshape.746 = bf16[1536,2048]{1,0:T(8,128)(2,1)} reshape(bf16[128,12,2048]{2,1,0:T(8,128)(2,1)} %all_to_all.32) | data formatting | bytes 12582912 | tf_op jit(solution)/shard_map/reshape | solution.py:215
  408.9 6.3 convolution_minimum_fusion
  415.2 5.0 fusion.7
  420.2 3.6 dot_general.53
  423.8 6.1 convert_bitcast_fusion
  429.9 65.9 %all_to_all.33 = bf16[4,1,32,12,2048]{4,2,3,1,0:T(8,128)(2,1)S(1)} all-to-all(bf16[4,1,32,12,2048]{4,2,3,1,0:T(8,128)(2,1)S(1)} %convert_bitcast_fusion), channel_id=1, replica_groups=mesh['grp'=2,'sp_0'=16,'sp_1'=2,'tp'=4] {'tp'}, dimensions={0} | all-to-all | bytes 12582912 | tf_op jit(solution)/shard_map/all_to_all | solution.py:59
  499.2 29.9 %all-to-all-start.5 = ((bf16[32,12,2048]{2,1,0:T(8,128)(2,1)}), bf16[32,12,2048]{2,1,0:T(8,128)(2,1)}, u32[]{:S(2)}, u32[]{:S(2)}) async-start(bf16[32,12,2048]{2,1,0:T(8,128)(2,1)} %copy.210), calls=%async_computation.5 | async-start | bytes 4194304 | tf_op jit(solution)/shard_map/all_to_all | solution.py:227
  529.3 98.1 %all-to-all-done.5 = bf16[32,12,2048]{2,1,0:T(8,128)(2,1)} async-done(((bf16[32,12,2048]{2,1,0:T(8,128)(2,1)}), bf16[32,12,2048]{2,1,0:T(8,128)(2,1)}, u32[]{:S(2)}, u32[]{:S(2)}) %all-to-all-start.5) | async-done | bytes 1572896 | tf_op jit(solution)/shard_map/all_to_all | solution.py:227
  627.4 3.6 reshape.748
  631.0 4.9 gather_fusion.1
  639.4 4.9 multiply_reduce_fusion
  (166 shorter events, 75.3 us)
Async XLA Ops:
  6.5 417.3 %copy-start = (bf16[1,512,2048]{2,1,0:T(8,128)(2,1)S(1)}, bf16[1,512,2048]{2,1,0:T(8,128)(2,1)}, u32[]{:S(2)}) copy-start(bf16[1,512,2048]{2,1,0:T(8,128)(2,1)} %param.33) | copy-start | bytes 6291460
  6.6 137.5 %all-gather.8.cloned.1.call-start = ((), (), s32[]{:S(2)}) async-start(), calls=%async_computation.6 | async-start | bytes 1114112 | tf_op jit(solution)/shard_map/all_gather | solution.py:36
  18.3 4.8 copy-start.31
  19.9 29.0 %copy-start.18 = (f32[512,4]{0,1:T(4,128)S(1)}, f32[512,4]{0,1:T(4,128)}, u32[]{:S(2)}) copy-start(f32[512,4]{0,1:T(4,128)} %param.24) | copy-start | bytes 24580
  22.2 31.8 %copy-start.7 = (bf16[512,256]{1,0:T(8,128)(2,1)S(1)}, bf16[512,256]{1,0:T(8,128)(2,1)}, u32[]{:S(2)}) copy-start(bf16[512,256]{1,0:T(8,128)(2,1)} %param.22) | copy-start | bytes 786436
  54.0 83.8 %copy-start.16 = (f32[1,4,4,128]{3,1,2,0:T(4,128)S(1)}, f32[1,4,4,128]{3,1,2,0:T(4,128)}, u32[]{:S(2)}) copy-start(f32[1,4,4,128]{3,1,2,0:T(4,128)} %copy-done.15) | copy-start | bytes 24580
  55.3 5.2 copy-start.32
  58.2 4.0 copy-start.11
  58.2 4.1 copy-start.12
  62.3 75.5 %copy-start.27 = (f32[4]{0:T(128)}, f32[4]{0:T(128)S(1)}, u32[]{:S(2)}) copy-start(f32[4]{0:T(128)S(1)} %get-tuple-element.66) | copy-start | bytes 52
  62.3 75.5 %copy-start.28 = (f32[4]{0:T(128)}, f32[4]{0:T(128)S(1)}, u32[]{:S(2)}) copy-start(f32[4]{0:T(128)S(1)} %get-tuple-element.67) | copy-start | bytes 52
  137.8 4.1 copy-start.14
  143.8 3.4 copy-start.8
  143.8 3.4 copy-start.9
  153.9 4.7 copy-start.19
  153.9 22.1 %copy-start.4 = (bf16[128,2048]{1,0:T(8,128)(2,1)S(1)}, bf16[128,2048]{1,0:T(8,128)(2,1)}, u32[]{:S(2)}) copy-start(bf16[128,2048]{1,0:T(8,128)(2,1)} %param.25) | copy-start | bytes 1572868
  153.9 20.0 %all-to-all-start = ((bf16[4,128,2048]{2,1,0:T(8,128)(2,1)}), bf16[4,128,2048]{2,1,0:T(8,128)(2,1)}, u32[]{:S(2)}, u32[]{:S(2)}) async-start(bf16[4,128,2048]{2,1,0:T(8,128)(2,1)} %bitcast.468), calls=%async_computation | async-start | bytes 4194304 | tf_op jit(solution)/shard_map/all_to_all | solution.py:59
  158.6 18.5 %copy-start.17 = (f32[2048]{0:T(1024)S(1)}, f32[2048]{0:T(1024)}, u32[]{:S(2)}) copy-start(f32[2048]{0:T(1024)} %param.28) | copy-start | bytes 24580
  408.9 6.3 copy-start.3
  408.9 6.3 copy-start.30
  497.0 32.1 %copy-start.29 = (f32[128,2]{0,1:T(2,128)S(1)}, f32[128,2]{0,1:T(2,128)}, u32[]{:S(2)}) copy-start(f32[128,2]{0,1:T(2,128)} %param.30) | copy-start | bytes 3076
  499.2 128.2 %all-to-all-start.5 = ((bf16[32,12,2048]{2,1,0:T(8,128)(2,1)}), bf16[32,12,2048]{2,1,0:T(8,128)(2,1)}, u32[]{:S(2)}, u32[]{:S(2)}) async-start(bf16[32,12,2048]{2,1,0:T(8,128)(2,1)} %copy.210), calls=%async_computation.5 | async-start | bytes 4194304 | tf_op jit(solution)/shard_map/all_to_all | solution.py:227
  635.9 8.4 %copy-start.2 = (f32[128,2048]{1,0:T(8,128)S(1)}, f32[128,2048]{1,0:T(8,128)}, u32[]{:S(2)}) copy-start(f32[128,2048]{1,0:T(8,128)} %copy-done.1) | copy-start | bytes 3145732
  639.4 4.9 copy-start.5
  (12 other events, 20.2 us)
Sparse Core Ops, SparseCore 0:
  49.0 54.4 all-gather.7
